TPU v7x, 32 devices: a whole 2x2x4 slice. The times are simulated.
32 devices in a mesh: rep: 4 (over z), fs: 4 (over y, x), tp: 2 (over core).
Axes of the slice: x: 2, y: 2, z: 4, core: 2. Of those that a mesh axis runs over, the one named last changes fastest.
Arguments:
- pre_gate: bfloat16 [3072, 7936], P('rep', ('fs', 'tp')), may hold values from -6 to 6
- pre_up: bfloat16 [3072, 7936], P('rep', ('fs', 'tp')), may hold values from -6 to 6
- cotangent: bfloat16 [3072, 4096], P('rep', ('fs', 'tp')), may hold values from -6 to 6
- down_weight: bfloat16 [7936, 4096], P(('fs', 'tp')), may hold values from -0.0625 to 0.0625
Outputs:
- grad_gate: bfloat16 [3072, 7936], P('rep', ('fs', 'tp'))
- grad_up: bfloat16 [3072, 7936], P('rep', ('fs', 'tp'))
- grad_down: float32 [7936, 4096], P(('fs', 'tp'), 'rep')
- row_squares: float32 [7936], P(('fs', 'tp'))
All inputs are finite; a program needn't handle non-finite values.
Results may differ from a plain program's by a relative error of at most 0.0034.
Values may be sent and summed in bfloat16 or wider, within the bound.
A program may use at most 128 MiB of HBM per device.

v0:
```python
import jax
import jax.numpy as jnp
from jax import lax
from jax.sharding import PartitionSpec as P


def local(pre_gate, pre_up, cotangent, down_weight):
    gate_wide = pre_gate.astype(jnp.float32)
    up_wide = pre_up.astype(jnp.float32)
    sigmoid_gate = jax.nn.sigmoid(gate_wide)
    act = gate_wide * sigmoid_gate
    hidden = (act * up_wide).astype(jnp.bfloat16)
    piece = lax.all_gather(cotangent, ("fs", "tp"), axis=1, tiled=True)
    partial_grad = lax.dot_general(
        piece, down_weight, (((1,), (1,)), ((), ())), preferred_element_type=jnp.float32
    )
    block = lax.dot_general(
        piece, hidden, (((0,), (0,)), ((), ())), preferred_element_type=jnp.float32
    )
    grad_up = (partial_grad * act).astype(jnp.bfloat16)
    slope = sigmoid_gate * (1.0 + gate_wide * (1.0 - sigmoid_gate))
    grad_gate = (partial_grad * up_wide * slope).astype(jnp.bfloat16)
    shard_rows = lax.psum_scatter(block, "rep", scatter_dimension=0, tiled=True)
    grad_down = shard_rows.T
    partial_squares = jnp.sum(grad_down * grad_down, axis=1)
    row_squares = lax.psum(partial_squares, "rep")
    return (grad_gate, grad_up, grad_down, row_squares)


def solution(mesh):
    placed = (
        P("rep", ("fs", "tp")),
        P("rep", ("fs", "tp")),
        P("rep", ("fs", "tp")),
        P(("fs", "tp"), None),
    )
    return jax.shard_map(
        local,
        mesh=mesh,
        in_specs=placed,
        out_specs=(
            P("rep", ("fs", "tp")),
            P("rep", ("fs", "tp")),
            P(("fs", "tp"), "rep"),
            P(("fs", "tp")),
        ),
        check_vma=False,
    )
```

profile of v0, /device:TPU:0, one launch (start us, length us, event | category | flops | bytes accessed | tf_op | source)
XLA Modules:
  0.0 365.5 jit_solution(954260564306209259)
XLA Ops:
  7.2 0.0 all-gather.2.cloned.1.call-start
  7.2 0.7 all-gather.2.cloned.1.call-update
  7.9 0.0 reduce-scatter.2.cloned.1.call-start
  7.9 51.2 %all-gather.2.cloned.1.call-done = bf16[768,4096]{1,0:T(8,128)(2,1)} async-done(((bf16[768,512]{1,0:T(8,128)(2,1)}), bf16[768,4096]{1,0:T(8,128)(2,1)}) %all-gather.2.cloned.1.call-update) | async-done | bytes 6291472 | tf_op jit(solution)/shard_map/all_gather | solution.py:13
  59.2 13.2 %convolution_bitcast_fusion = f32[4096,992]{0,1:T(8,128)} fusion(bf16[768,4096]{1,0:T(8,128)(2,1)} %all-gather.2.cloned.1.call-done, bf16[768,992]{0,1:T(8,128)(2,1)} %param.5, bf16[768,992]{0,1:T(8,128)(2,1)} %param.4), kind=kOutput, calls=%fused_computation | convolution fusion | flops 6247219200 | bytes 25591808 | tf_op jit(solution)/shard_map/dot_general | solution.py:17
  72.3 0.0 copy-start
  72.3 0.0 copy-start.1
  72.3 0.0 reduce-scatter.2.cloned.1.call-update
  72.4 1.4 copy-done
  73.7 0.5 copy-done.1
  74.2 12.8 %multiply_convert_fusion = (bf16[768,992]{0,1:T(8,128)(2,1)}, bf16[768,992]{0,1:T(8,128)(2,1)}) fusion(bf16[768,992]{0,1:T(8,128)(2,1)S(1)} %copy-done, bf16[768,992]{0,1:T(8,128)(2,1)S(1)} %copy-done.1, bf16[768,4096]{1,0:T(8,128)(2,1)} %all-gather.2.cloned.1.call-done, bf16[992,4096]{1,0:T(8,128)(2,1)} %param.7), kind=kOutput, calls=%fused_computation.15 | convolution fusion | flops 6252552192 | bytes 20512768 | tf_op jit(solution)/shard_map/dot_general | solution.py:14
  87.0 257.7 %reduce-scatter.2.cloned.1.call-done = f32[1024,992]{0,1:T(8,128)} async-done(((f32[4096,992]{0,1:T(8,128)}), f32[1024,992]{0,1:T(8,128)}) %reduce-scatter.2.cloned.1.call-update) | async-done | bytes 4063248 | tf_op jit(solution)/shard_map/reduce_scatter | solution.py:23
  344.6 2.5 multiply_reduce_fusion
  347.1 11.6 %psum.7 = f32[992]{0:T(1024)} all-reduce(f32[992]{0:T(1024)S(1)} %multiply_reduce_fusion), channel_id=1, replica_groups=mesh['rep'=4,'fs'=4,'tp'=2] {'rep'}, use_global_device_ids=true, to_apply=%region_2.0 | all-reduce | flops 992 | bytes 7936 | tf_op jit(solution)/shard_map/psum | solution.py:26
Async XLA Ops:
  7.2 52.0 %all-gather.2.cloned.1.call-start = ((), (), s32[]{:S(2)}) async-start(), calls=%async_computation.1 | async-start | bytes 7077888 | tf_op jit(solution)/shard_map/all_gather | solution.py:13
  7.9 336.7 %reduce-scatter.2.cloned.1.call-start = ((), (), s32[]{:S(2)}) async-start(), calls=%async_computation.2 | async-start | bytes 20316160 | tf_op jit(solution)/shard_map/reduce_scatter | solution.py:23
  72.3 1.4 copy-start
  72.3 1.8 copy-start.1
Sparse Core Ops, SparseCore 0:
  9.8 49.2 all-gather.1
  72.5 272.0 reduce-scatter.1
where the time goes:
time: 366 us
  waiting for transfers between devices  310 us (85%)
  matrix products  25.9 us (7%)
  between operations  14 us (4%)
  blocking collectives  11.6 us (3%)
    reduce_scatter x1, waiting for transfers between devices, local(): shard_rows = lax.psum_scatter(block, 'rep', scatter_dimension=0, tiled=True)  258 us
    all_gather x1, waiting for transfers between devices, local(): piece = lax.all_gather(cotangent, ('fs', 'tp'), axis=1, tiled=True)  51.2 us
    dot_general x1, matrix products, local(): lax.dot_general(piece, hidden, (((0,), (0,)), ((), ())), preferred_elemen...  13.2 us
    dot_general x1, matrix products, local(): lax.dot_general(piece, down_weight, (((1,), (1,)), ((), ())), preferred_e...  12.8 us
    psum x1, blocking collectives, local(): row_squares = lax.psum(partial_squares, 'rep')  11.6 us
  transfers between devices with their start and end apart: 2, of which 2 were waited for; matrix products, arithmetic and copies ran while one was open for 3% of the time, Pallas kernels for 0%

commit v1 on v0

v1 whole, which is shorter than its diff:
```python
import jax
import jax.numpy as jnp
from jax import lax
from jax.experimental import pallas as pl
from jax.experimental.pallas import tpu as pltpu
from jax.sharding import PartitionSpec as P

MESH = pl.DeviceIdType.MESH
F32 = jnp.float32
BF16 = jnp.bfloat16


def local(pre_gate, pre_up, cotangent, down_weight):
    gate_wide = pre_gate.astype(F32)
    up_wide = pre_up.astype(F32)
    sigmoid_gate = jax.nn.sigmoid(gate_wide)
    act = gate_wide * sigmoid_gate
    hidden = (act * up_wide).astype(BF16)
    piece = lax.all_gather(cotangent, ("fs", "tp"), axis=1, tiled=True)
    partial_grad = lax.dot_general(
        piece, down_weight, (((1,), (1,)), ((), ())), preferred_element_type=F32
    )
    block = lax.dot_general(
        piece, hidden, (((0,), (0,)), ((), ())), preferred_element_type=F32
    )
    grad_up = (partial_grad * act).astype(BF16)
    slope = sigmoid_gate * (1.0 + gate_wide * (1.0 - sigmoid_gate))
    grad_gate = (partial_grad * up_wide * slope).astype(BF16)
    shard_rows = lax.psum_scatter(block, "rep", scatter_dimension=0, tiled=True)
    grad_down = shard_rows.T
    row_squares = lax.psum(jnp.sum(grad_down * grad_down, axis=1), "rep")
    return (grad_gate, grad_up, grad_down, row_squares)


CHUNKS = 4
OWN, G0, G1, G2 = 0, 7, 14, 21
ZX0, ZX1, ZY, ZF = 28, 29, 31, 33
HO_S = 34
HM_S = HO_S + CHUNKS
HF_S = HM_S + CHUNKS
C_S = HF_S + CHUNKS
N_SEM = C_S + CHUNKS


def chunk_rows(rows):
    step = -(-rows // CHUNKS)
    step = -(-step // 16) * 16
    return [(a, min(step, rows - a)) for a in range(0, rows, step)]


def kernel(gate, up, shard, w, hid, gg, gu, out,
           G, X, Y, HO, HM, HF, CS, CR, ssem, rsem):
    rep = lax.axis_index("rep")
    fs = lax.axis_index("fs")
    tp = lax.axis_index("tp")
    tokens, wide = shard.shape
    rows = hid.shape[0]
    cols = out.shape[1]
    sub = Y.shape[2]
    x, y = fs % 2, fs // 2
    peers = (y * 2 + (1 - x), (1 - y) * 2 + x, (1 - y) * 2 + (1 - x))
    me = fs * 2 + tp
    side = rep // 2
    inner = (rep == 1) | (rep == 2)
    outer = (rep == 0) | (rep == 3)
    mid = 3 - rep
    edge = side * 3
    inn = 1 + side
    other = 1 - side
    partner = (rep, fs, 1 - tp)
    parts = chunk_rows(rows)

    def copy(src, dst, i, dev):
        return pltpu.make_async_remote_copy(
            src_ref=src, dst_ref=dst, send_sem=ssem.at[i], recv_sem=rsem.at[i],
            device_id=dev, device_id_type=MESH)

    def at(start, size):
        return pl.ds(pl.multiple_of(start, 128), size)

    barrier = pltpu.get_barrier_semaphore()

    def hello(dev):
        pl.semaphore_signal(barrier, inc=1, device_id=dev, device_id_type=MESH)

    for q in peers:
        hello((rep, q, tp))
    hello(partner)

    @pl.when(outer)
    def _():
        hello((inn, fs, tp))
        pl.semaphore_wait(barrier, 5)

    @pl.when(inner)
    def _():
        hello((mid, fs, tp))
        hello((edge, fs, tp))
        pl.semaphore_wait(barrier, 6)

    def send_plane(base, src, view):
        for k, q in enumerate(peers):
            copy(src, view(me), base + k, (rep, q, tp)).start()
        copy(src, view(me), base + 3, partner).start()

    def relay_plane(base, view):
        for k, q in enumerate(peers):
            v = view(q * 2 + tp)
            copy(v, v, base + k, partner).wait_recv()
            copy(v, v, base + 4 + k, partner).start()

    def finish_plane(base, view):
        v = view(fs * 2 + 1 - tp)
        copy(v, v, base + 3, partner).wait_recv()
        for k, q in enumerate(peers):
            v = view(q * 2 + 1 - tp)
            copy(v, v, base + 4 + k, partner).wait_recv()

    def sent_plane(base, view):
        for k in range(7):
            copy(view(me), view(me), base + k, partner).wait_send()

    def own_view(p):
        return G.at[:, at(p * wide, wide)]

    def x_view(u, n):
        return lambda p: X.at[pl.ds(u, n), :, at(p * sub, sub)]

    def unit(u):
        return X.at[u, :, at(me * sub, sub)]

    def gcol(c):
        return G.at[:, at(c * cols + me * sub, sub)]

    v0, v1, v2 = x_view(0, 1), x_view(1, 2), x_view(3, 2)

    send_plane(OWN, shard, own_view)

    @pl.when(outer)
    def _():
        for c, (a, n) in enumerate(parts):
            copy(hid.at[pl.ds(a, n)], HO.at[pl.ds(a, n)], HO_S + c, (inn, fs, tp)).start()

    @pl.when(inner)
    def _():
        for c, (a, n) in enumerate(parts):
            copy(hid.at[pl.ds(a, n)], HM.at[pl.ds(a, n)], HM_S + c, (mid, fs, tp)).start()

    G[:, at(me * wide, wide)] = shard[...]
    relay_plane(OWN, own_view)
    finish_plane(OWN, own_view)

    def hidden_grads():
        tile = 256

        @pl.loop(0, tokens // tile)
        def _(t):
            r = pl.ds(pl.multiple_of(t * tile, tile), tile)
            pg = lax.dot_general(G[r, :], w[...], (((1,), (1,)), ((), ())),
                                 preferred_element_type=F32)
            g = gate[r, :].astype(F32)
            u = up[r, :].astype(F32)
            s = 1.0 / (1.0 + jnp.exp(-g))
            gu[r, :] = (pg * (g * s)).astype(BF16)
            gg[r, :] = (pg * u * (s * (1.0 + g * (1.0 - s)))).astype(BF16)

    def dot(h, a, n, b):
        return jnp.dot(h[pl.ds(a, n), :], b, preferred_element_type=F32)

    @pl.when(outer)
    def _():
        to = (inn, fs, tp)
        for j in range(2):
            copy(gcol(other * 2 + j), Y.at[j], ZY + j, to).start()
        copy(gcol(inn), unit(0), ZX0, to).start()
        hidden_grads()
        for c, (a, n) in enumerate(parts):
            out[pl.ds(a, n), :] = dot(hid, a, n, G[:, at(rep * cols, cols)])
        for c, (a, n) in enumerate(parts):
            r = pl.ds(a, n)
            copy(CS.at[r], CR.at[r], C_S + c, to).wait_recv()
            out[r, :] = out[r, :] + CR[r, :].astype(F32)
        for c, (a, n) in enumerate(parts):
            copy(hid.at[pl.ds(a, n)], HO.at[pl.ds(a, n)], HO_S + c, to).wait_send()
        for j in range(2):
            copy(Y.at[j], Y.at[j], ZY + j, to).wait_send()
        copy(unit(0), unit(0), ZX0, to).wait_send()

    @pl.when(inner)
    def _():
        to = (mid, fs, tp)
        back = (edge, fs, tp)
        for j in range(2):
            copy(gcol(other * 2 + j), unit(1 + j), ZX1 + j, to).start()

        def forward(c):
            a, n = parts[c]
            v = HO.at[pl.ds(a, n)]
            copy(v, v, HO_S + c, to).wait_recv()
            copy(v, HF.at[pl.ds(a, n)], HF_S + c, to).start()

        forward(0)
        for j in range(2):
            copy(Y.at[j], Y.at[j], ZY + j, to).wait_recv()
        copy(Y, v2(me), ZF, to).start()
        for c in range(1, len(parts)):
            forward(c)
        for j in range(2):
            copy(unit(1 + j), unit(1 + j), ZX1 + j, to).wait_recv()
        send_plane(G1, v1(me), v1)
        copy(unit(0), unit(0), ZX0, to).wait_recv()
        send_plane(G0, v0(me), v0)
        relay_plane(G1, v1)
        relay_plane(G0, v0)
        hidden_grads()
        copy(v2(me), v2(me), ZF, to).wait_recv()
        send_plane(G2, v2(me), v2)
        finish_plane(G1, v1)
        finish_plane(G0, v0)
        relay_plane(G2, v2)
        finish_plane(G2, v2)
        jr = rep % 2
        je = 1 - jr
        for c, (a, n) in enumerate(parts):
            r = pl.ds(a, n)
            copy(HM.at[r], HM.at[r], HM_S + c, to).wait_recv()
            copy(HF.at[r], HF.at[r], HF_S + c, to).wait_recv()
            total = dot(hid, a, n, G[:, at(edge * cols, cols)])
            total = total + dot(HM, a, n, X[1 + je])
            total = total + dot(HF, a, n, X[3 + je])
            CS[r, :] = total.astype(BF16)
            copy(CS.at[r], CR.at[r], C_S + c, back).start()
        for c, (a, n) in enumerate(parts):
            total = dot(hid, a, n, G[:, at(rep * cols, cols)])
            total = total + dot(HO, a, n, X[0])
            total = total + dot(HM, a, n, X[1 + jr])
            total = total + dot(HF, a, n, X[3 + jr])
            out[pl.ds(a, n), :] = total
        for j in range(2):
            copy(unit(1 + j), unit(1 + j), ZX1 + j, to).wait_send()
        copy(Y, v2(me), ZF, to).wait_send()
        for c, (a, n) in enumerate(parts):
            r = pl.ds(a, n)
            copy(HM.at[r], HM.at[r], HM_S + c, to).wait_send()
            copy(HF.at[r], HF.at[r], HF_S + c, to).wait_send()
            copy(CS.at[r], CS.at[r], C_S + c, back).wait_send()
        sent_plane(G0, v0)
        sent_plane(G1, v1)
        sent_plane(G2, v2)

    sent_plane(OWN, own_view)


def fused(pre_gate, pre_up, cotangent, down_weight):
    tokens, rows = pre_gate.shape
    width = down_weight.shape[1]
    reps = lax.axis_size("rep")
    plane = width // cotangent.shape[1]
    cols = width // reps
    g = pre_gate.astype(F32)
    hid = (g * jax.nn.sigmoid(g) * pre_up.astype(F32)).astype(BF16).T
    vmem = pl.BlockSpec(memory_space=pltpu.VMEM)
    hid_buf = pltpu.VMEM((rows, tokens), BF16)
    gg, gu, out = pl.pallas_call(
        kernel,
        out_shape=(
            jax.ShapeDtypeStruct((tokens, rows), BF16),
            jax.ShapeDtypeStruct((tokens, rows), BF16),
            jax.ShapeDtypeStruct((rows, cols), F32),
        ),
        in_specs=[vmem] * 5,
        out_specs=(vmem,) * 3,
        scratch_shapes=[
            pltpu.VMEM((tokens, width), BF16),
            pltpu.VMEM((5, tokens, cols), BF16),
            pltpu.VMEM((2, tokens, cols // plane), BF16),
            hid_buf, hid_buf, hid_buf,
            pltpu.VMEM((rows, cols), BF16),
            pltpu.VMEM((rows, cols), BF16),
            pltpu.SemaphoreType.DMA((N_SEM,)),
            pltpu.SemaphoreType.DMA((N_SEM,)),
        ],
        compiler_params=pltpu.CompilerParams(
            collective_id=0, has_side_effects=True, vmem_limit_bytes=67043328),
    )(pre_gate, pre_up, cotangent, down_weight, hid)
    row_squares = lax.psum(jnp.sum(out * out, axis=1), "rep")
    return gg, gu, out, row_squares


def solution(mesh):
    placed = (
        P("rep", ("fs", "tp")),
        P("rep", ("fs", "tp")),
        P("rep", ("fs", "tp")),
        P(("fs", "tp"), None),
    )
    shape = dict(mesh.shape)
    fits = shape["rep"] // 2 == 2 and shape["fs"] // 2 == 2 and shape["tp"] == 2
    return jax.shard_map(
        fused if fits else local,
        mesh=mesh,
        in_specs=placed,
        out_specs=(
            P("rep", ("fs", "tp")),
            P("rep", ("fs", "tp")),
            P(("fs", "tp"), "rep"),
            P(("fs", "tp")),
        ),
        check_vma=False,
    )
```

time: 366 us -> 195 us (0.53)
  waiting for transfers between devices: 310 us -> 0 us
  Pallas kernels: 0 us -> 164 us
  matrix products: 25.9 us -> 0 us
  between operations: 14 us -> 0.67 us
  local copies, waits for them, and re-layouts: 1.82 us -> 12.3 us
  other arithmetic: 2.48 us -> 6.53 us
    reduce_scatter x1 -> x0, waiting for transfers between devices: 258 us -> none  [local(): shard_rows = lax.psum_scatter(block, 'rep', scatter_dimension=0, tiled=True)]
    pallas_call x0 -> x1, Pallas kernels: none -> 164 us  [fused(): pl.pallas_call(kernel, out_shape=(jax.ShapeDtypeStruct((tokens, rows), BF...]
    all_gather x1 -> x0, waiting for transfers between devices: 51.2 us -> none  [local(): piece = lax.all_gather(cotangent, ('fs', 'tp'), axis=1, tiled=True)]
    dot_general x2 -> x0, matrix products: 25.9 us -> none  [the longest x1 13.2 us: local(): lax.dot_general(piece, hidden, (((0,), (0,)), ((), ())), preferred_elemen...]
    unnamed x4 -> x11, local copies, waits for them, and re-layouts: 1.82 us -> 12.3 us
    transpose x0 -> x1, other arithmetic: none -> 4.05 us  [fused(): hid = (g * jax.nn.sigmoid(g) * pre_up.astype(F32)).astype(BF16).T]
  transfers between devices with their start and end apart: 2 -> 0, of which waited for: 2 -> 0; matrix products, arithmetic and copies ran while one was open for 3% -> 0% of each run, Pallas kernels for 0% -> 0%
where the time goes in v1:
time: 195 us
  Pallas kernels  164 us (84%)
  local copies, waits for them, and re-layouts  12.3 us (6%)
  blocking collectives  11.6 us (6%)
  other arithmetic  6.53 us (3%)
    pallas_call x1, Pallas kernels, fused(): pl.pallas_call(kernel, out_shape=(jax.ShapeDtypeStruct((tokens, rows), BF...  164 us
    unnamed x11, local copies, waits for them, and re-layouts  12.3 us
    psum x1, blocking collectives, fused(): row_squares = lax.psum(jnp.sum(out * out, axis=1), 'rep')  11.6 us
    transpose x1, other arithmetic, fused(): hid = (g * jax.nn.sigmoid(g) * pre_up.astype(F32)).astype(BF16).T  4.05 us

profile of v1, /device:TPU:0, one launch (start us, length us, event | category | flops | bytes accessed | tf_op | source)
XLA Modules:
  0.0 194.9 jit_solution(6562419156293417214)
XLA Ops:
  0.6 0.0 copy-start.1
  0.6 0.0 copy-start
  0.7 4.1 %fusion.5.hid = bf16[992,768]{1,0:T(8,128)(2,1)} fusion(bf16[768,992]{0,1:T(8,128)(2,1)} %param.5, bf16[768,992]{0,1:T(8,128)(2,1)} %param.4), kind=kLoop, calls=%fused_computation.8 | loop fusion | flops 6094848 | bytes 4571136 | tf_op jit(solution)/shard_map/transpose | solution.py:261
  4.7 0.0 copy-done
  4.7 1.6 copy.8.gate
  6.3 0.0 copy-done.1
  6.3 1.6 copy.9.up
  8.0 163.8 %shard_map.75 = (bf16[768,992]{1,0:T(8,128)(2,1)}, bf16[768,992]{1,0:T(8,128)(2,1)}, f32[992,1024]{1,0:T(8,128)}) custom-call(bf16[768,992]{1,0:T(8,128)(2,1)} %copy.8.gate, bf16[768,992]{1,0:T(8,128)(2,1)} %copy.9.up, bf16[768,512]{1,0:T(8,128)(2,1)} %shard.1, bf16[992,4096]{1,0:T(8,128)(2,1)} %w.1, bf16[992,768]{1,0:T(8,128)(2,1)} %fusion.5.hid), custom_call_target="tpu_custom_call" | custom-call | tf_op jit(solution)/shard_map/pallas_call | solution.py:264
  171.8 0.0 copy-start.2
  171.8 2.7 %copy.10 = bf16[768,992]{0,1:T(8,128)(2,1)} copy(bf16[768,992]{1,0:T(8,128)(2,1)} %get-tuple-element.10) | data formatting | bytes 3047424
  174.5 2.5 %multiply_reduce_fusion = f32[992]{0:T(1024)S(1)} fusion(f32[992,1024]{1,0:T(8,128)} %get-tuple-element.20), kind=kLoop, calls=%fused_computation | loop fusion | flops 2030624 | bytes 4067200 | tf_op jit(solution)/shard_map/reduce_sum | solution.py:286
  177.0 11.6 %psum.7 = f32[992]{0:T(1024)} all-reduce(f32[992]{0:T(1024)S(1)} %multiply_reduce_fusion), channel_id=1, replica_groups=mesh['rep'=4,'fs'=4,'tp'=2] {'rep'}, use_global_device_ids=true, to_apply=%region_1.0 | all-reduce | flops 992 | bytes 7936 | tf_op jit(solution)/shard_map/psum | solution.py:286
  188.6 0.0 copy-done.2
  188.6 1.6 copy.11
  190.2 4.7 %copy.13 = f32[992,1024]{1,0:T(8,128)} copy(f32[992,1024]{1,0:T(8,128)} %get-tuple-element.20) | data formatting | bytes 8126464
Async XLA Ops:
  0.6 5.7 %copy-start.1 = (bf16[768,992]{0,1:T(8,128)(2,1)S(1)}, bf16[768,992]{0,1:T(8,128)(2,1)}, u32[]{:S(2)}) copy-start(bf16[768,992]{0,1:T(8,128)(2,1)} %param.5) | copy-start | bytes 4571140
  0.6 4.1 %copy-start = (bf16[768,992]{0,1:T(8,128)(2,1)S(1)}, bf16[768,992]{0,1:T(8,128)(2,1)}, u32[]{:S(2)}) copy-start(bf16[768,992]{0,1:T(8,128)(2,1)} %param.4) | copy-start | bytes 4571140
  171.8 16.9 %copy-start.2 = (bf16[768,992]{1,0:T(8,128)(2,1)S(1)}, bf16[768,992]{1,0:T(8,128)(2,1)}, u32[]{:S(2)}) copy-start(bf16[768,992]{1,0:T(8,128)(2,1)} %get-tuple-element.11) | copy-start | bytes 4571140

commit v2 on v1

v2 whole, which is shorter than its diff:
```python
import jax
import jax.numpy as jnp
from jax import lax
from jax.experimental import pallas as pl
from jax.experimental.pallas import tpu as pltpu
from jax.sharding import PartitionSpec as P

MESH = pl.DeviceIdType.MESH
F32 = jnp.float32
BF16 = jnp.bfloat16


def local(pre_gate, pre_up, cotangent, down_weight):
    gate_wide = pre_gate.astype(F32)
    up_wide = pre_up.astype(F32)
    sigmoid_gate = jax.nn.sigmoid(gate_wide)
    act = gate_wide * sigmoid_gate
    hidden = (act * up_wide).astype(BF16)
    piece = lax.all_gather(cotangent, ("fs", "tp"), axis=1, tiled=True)
    partial_grad = lax.dot_general(
        piece, down_weight, (((1,), (1,)), ((), ())), preferred_element_type=F32
    )
    block = lax.dot_general(
        piece, hidden, (((0,), (0,)), ((), ())), preferred_element_type=F32
    )
    grad_up = (partial_grad * act).astype(BF16)
    slope = sigmoid_gate * (1.0 + gate_wide * (1.0 - sigmoid_gate))
    grad_gate = (partial_grad * up_wide * slope).astype(BF16)
    shard_rows = lax.psum_scatter(block, "rep", scatter_dimension=0, tiled=True)
    grad_down = shard_rows.T
    row_squares = lax.psum(jnp.sum(grad_down * grad_down, axis=1), "rep")
    return (grad_gate, grad_up, grad_down, row_squares)


CHUNKS = 4
OWN, G0, G1E, G1R, G2E, G2R = (8 * i for i in range(6))
ZX, ZM, ZY, ZF, SQ_S = 48, 49, 51, 53, 55
HO_S = 58
HM_S = HO_S + CHUNKS
HF_S = HM_S + CHUNKS
C_S = HF_S + CHUNKS
N_SEM = C_S + CHUNKS


def chunk_rows(rows):
    step = -(-rows // CHUNKS)
    step = -(-step // 16) * 16
    return [(a, min(step, rows - a)) for a in range(0, rows, step)]


def kernel(gate_in, up_in, shard, w_in, hid, gg_out, gu_out, out_out, sq_out,
           G, X, Y, HO, HM, HF, CS, CR, gate, up, w, gg, gu, out, acc, SQ,
           ssem, rsem, lsem):
    rep = lax.axis_index("rep")
    fs = lax.axis_index("fs")
    tp = lax.axis_index("tp")
    tokens, wide = shard.shape
    rows = hid.shape[0]
    cols = out.shape[1]
    sub = Y.shape[2]
    half = tokens // 2
    x, y = fs % 2, fs // 2
    xq, yq, dq = y * 2 + (1 - x), (1 - y) * 2 + x, (1 - y) * 2 + (1 - x)
    me = fs * 2 + tp
    side = rep // 2
    inner = (rep == 1) | (rep == 2)
    outer = (rep == 0) | (rep == 3)
    mid = 3 - rep
    edge = side * 3
    inn = 1 + side
    far_edge = (1 - side) * 3
    far_inn = 2 - side
    partner = (rep, fs, 1 - tp)
    parts = chunk_rows(rows)
    early = range(len(parts) - 1)
    last = len(parts) - 1

    def copy(src, dst, i, dev):
        return pltpu.make_async_remote_copy(
            src_ref=src, dst_ref=dst, send_sem=ssem.at[i], recv_sem=rsem.at[i],
            device_id=dev, device_id_type=MESH)

    def at(start, size):
        return pl.ds(pl.multiple_of(start, 128), size)

    loads = [pltpu.make_async_copy(a, b, lsem.at[i])
             for i, (a, b) in enumerate([(gate_in, gate), (up_in, up), (w_in, w)])]
    for load in loads:
        load.start()

    barrier = pltpu.get_barrier_semaphore()

    def hello(dev):
        pl.semaphore_signal(barrier, inc=1, device_id=dev, device_id_type=MESH)

    for d in range(1, 4):
        hello(((rep + d) % 4, fs, tp))
    for q in (xq, yq):
        hello((rep, q, tp))
    hello(partner)
    pl.semaphore_wait(barrier, 6)

    def send_plane(base, src, view):
        copy(src, view(me), base, (rep, xq, tp)).start()
        copy(src, view(me), base + 1, (rep, yq, tp)).start()
        copy(src, view(me), base + 4, partner).start()

    def top(v):
        return v.at[pl.ds(0, half)]

    def low(v):
        return v.at[pl.ds(half, half)]

    def relay_plane(base, view):
        vx, vy, vd = view(xq * 2 + tp), view(yq * 2 + tp), view(dq * 2 + tp)
        copy(vx, vx, base, partner).wait_recv()
        copy(top(vx), top(vx), base + 2, (rep, yq, tp)).start()
        copy(vx, vx, base + 5, partner).start()
        copy(vy, vy, base + 1, partner).wait_recv()
        copy(low(vy), low(vy), base + 3, (rep, xq, tp)).start()
        copy(vy, vy, base + 6, partner).start()
        copy(top(vd), top(vd), base + 2, partner).wait_recv()
        copy(low(vd), low(vd), base + 3, partner).wait_recv()
        copy(vd, vd, base + 7, partner).start()

    def finish_plane(base, view):
        for k, q in ((4, fs), (5, xq), (6, yq), (7, dq)):
            v = view(q * 2 + 1 - tp)
            copy(v, v, base + k, partner).wait_recv()

    def sent_plane(base, view):
        v = view(me)
        for k in range(8):
            u = top(v) if k in (2, 3) else v
            copy(u, u, base + k, partner).wait_send()

    def own_view(p):
        return G.at[:, at(p * wide, wide)]

    def x_view(u):
        return lambda p: X.at[u, :, at(p * sub, sub)]

    def gcol(c):
        return G.at[:, at(c * cols + me * sub, sub)]

    x_o, m_e, m_r, f_e, f_r = (x_view(u) for u in range(5))

    def chunk(ref, c):
        a, n = parts[c]
        return ref.at[pl.ds(a, n)]

    send_plane(OWN, shard, own_view)

    @pl.when(outer)
    def _():
        for c in early:
            copy(chunk(hid, c), chunk(HO, c), HO_S + c, (inn, fs, tp)).start()

    @pl.when(inner)
    def _():
        for c in early:
            copy(chunk(hid, c), chunk(HM, c), HM_S + c, (mid, fs, tp)).start()

    G[:, at(me * wide, wide)] = shard[...]
    relay_plane(OWN, own_view)
    finish_plane(OWN, own_view)

    def hidden_grads():
        for load in loads:
            load.wait()
        tile = rows // 2

        @pl.loop(0, 2)
        def _(t):
            r = pl.ds(pl.multiple_of(t * tile, 16), tile)
            pg = lax.dot_general(w[r, :], G[...], (((1,), (1,)), ((), ())),
                                 preferred_element_type=F32)
            g = gate[r, :].astype(F32)
            u = up[r, :].astype(F32)
            s = 1.0 / (1.0 + jnp.exp(-g))
            gu[r, :] = (pg * (g * s)).astype(BF16)
            gg[r, :] = (pg * u * (s * (1.0 + g * (1.0 - s)))).astype(BF16)

        pltpu.make_async_copy(gg, gg_out, lsem.at[3]).start()
        pltpu.make_async_copy(gu, gu_out, lsem.at[4]).start()

    def dot(h, c, b):
        a, n = parts[c]
        return jnp.dot(h[pl.ds(a, n), :], b, preferred_element_type=F32)

    def store(c, total):
        a, n = parts[c]
        r = pl.ds(a, n)
        out[r, :] = total
        pltpu.make_async_copy(chunk(out, c), chunk(out_out, c), lsem.at[5 + c]).start()
        square = total * total
        lanes = square[:, 0:128]
        for k in range(1, cols // 128):
            lanes = lanes + square[:, k * 128:(k + 1) * 128]
        acc[r, :] = lanes

    acc[...] = jnp.zeros_like(acc)

    @pl.when(outer)
    def _():
        to = (inn, fs, tp)
        copy(gcol(far_edge), Y.at[0], ZY, to).start()
        copy(gcol(far_inn), Y.at[1], ZY + 1, to).start()
        copy(chunk(hid, last), chunk(HO, last), HO_S + last, to).start()
        copy(gcol(inn), x_o(me), ZX, to).start()
        hidden_grads()
        for c in range(len(parts)):
            a, n = parts[c]
            out[pl.ds(a, n), :] = dot(hid, c, G[:, at(rep * cols, cols)])
        for c in range(len(parts)):
            a, n = parts[c]
            copy(chunk(CS, c), chunk(CR, c), C_S + c, to).wait_recv()
            store(c, out[pl.ds(a, n), :] + CR[pl.ds(a, n), :].astype(F32))
        for c in range(len(parts)):
            copy(chunk(hid, c), chunk(HO, c), HO_S + c, to).wait_send()
        for j in range(2):
            copy(Y.at[j], Y.at[j], ZY + j, to).wait_send()
        copy(x_o(me), x_o(me), ZX, to).wait_send()

    @pl.when(inner)
    def _():
        to = (mid, fs, tp)
        back = (edge, fs, tp)

        def forward(c):
            copy(chunk(HO, c), chunk(HO, c), HO_S + c, to).wait_recv()
            copy(chunk(HO, c), chunk(HF, c), HF_S + c, to).start()

        def arrived(view, i):
            copy(view(me), view(me), i, to).wait_recv()

        copy(gcol(far_edge), m_e(me), ZM, to).start()
        copy(Y.at[0], Y.at[0], ZY, to).wait_recv()
        copy(Y.at[0], f_e(me), ZF, to).start()
        forward(0)
        arrived(m_e, ZM)
        send_plane(G1E, m_e(me), m_e)
        for c in early:
            if c:
                forward(c)
        copy(gcol(mid), m_r(me), ZM + 1, to).start()
        arrived(f_e, ZF)
        send_plane(G2E, f_e(me), f_e)
        copy(Y.at[1], Y.at[1], ZY + 1, to).wait_recv()
        copy(Y.at[1], f_r(me), ZF + 1, to).start()
        copy(chunk(hid, last), chunk(HM, last), HM_S + last, to).start()
        relay_plane(G1E, m_e)
        relay_plane(G2E, f_e)
        forward(last)
        arrived(x_o, ZX)
        send_plane(G0, x_o(me), x_o)
        finish_plane(G1E, m_e)
        finish_plane(G2E, f_e)

        def give(c):
            a, n = parts[c]
            copy(chunk(HM, c), chunk(HM, c), HM_S + c, to).wait_recv()
            copy(chunk(HF, c), chunk(HF, c), HF_S + c, to).wait_recv()
            total = dot(hid, c, G[:, at(edge * cols, cols)])
            total = total + dot(HM, c, X[1])
            total = total + dot(HF, c, X[3])
            CS[pl.ds(a, n), :] = total.astype(BF16)
            copy(chunk(CS, c), chunk(CR, c), C_S + c, back).start()

        for c in early:
            give(c)
        relay_plane(G0, x_o)
        arrived(m_r, ZM + 1)
        send_plane(G1R, m_r(me), m_r)
        arrived(f_r, ZF + 1)
        send_plane(G2R, f_r(me), f_r)
        hidden_grads()
        relay_plane(G1R, m_r)
        relay_plane(G2R, f_r)
        give(last)
        finish_plane(G0, x_o)
        finish_plane(G1R, m_r)
        finish_plane(G2R, f_r)
        for c in range(len(parts)):
            total = dot(hid, c, G[:, at(rep * cols, cols)])
            total = total + dot(HO, c, X[0])
            total = total + dot(HM, c, X[2])
            total = total + dot(HF, c, X[4])
            store(c, total)
        for j in range(2):
            copy(Y.at[j], Y.at[j], ZM + j, to).wait_send()
            copy(Y.at[j], Y.at[j], ZF + j, to).wait_send()
        for c in range(len(parts)):
            copy(chunk(HM, c), chunk(HM, c), HM_S + c, to).wait_send()
            copy(chunk(HF, c), chunk(HF, c), HF_S + c, to).wait_send()
            copy(chunk(CS, c), chunk(CS, c), C_S + c, back).wait_send()
        sent_plane(G0, x_o)
        sent_plane(G1E, m_e)
        sent_plane(G1R, m_r)
        sent_plane(G2E, f_e)
        sent_plane(G2R, f_r)

    sums = jnp.sum(acc[...].T, axis=0, keepdims=True)
    SQ[rep] = jnp.broadcast_to(sums, SQ.shape[1:])
    for d in range(1, 4):
        copy(SQ.at[rep], SQ.at[rep], SQ_S + d - 1, ((rep + d) % 4, fs, tp)).start()
    for d in range(1, 4):
        v = SQ.at[(rep + 4 - d) % 4]
        copy(v, v, SQ_S + d - 1, partner).wait_recv()
    sq_out[...] = (SQ[0] + SQ[1]) + (SQ[2] + SQ[3])
    for d in range(1, 4):
        copy(SQ.at[rep], SQ.at[rep], SQ_S + d - 1, partner).wait_send()
    sent_plane(OWN, own_view)
    pltpu.make_async_copy(gg, gg_out, lsem.at[3]).wait()
    pltpu.make_async_copy(gu, gu_out, lsem.at[4]).wait()
    for c in range(len(parts)):
        pltpu.make_async_copy(chunk(out, c), chunk(out_out, c), lsem.at[5 + c]).wait()


def fused(pre_gate, pre_up, cotangent, down_weight):
    tokens, rows = pre_gate.shape
    width = down_weight.shape[1]
    reps = lax.axis_size("rep")
    plane = width // cotangent.shape[1]
    cols = width // reps
    padded = -(-rows // 128) * 128
    gate_t, up_t = pre_gate.T, pre_up.T
    g = gate_t.astype(F32)
    hid = (g * jax.nn.sigmoid(g) * up_t.astype(F32)).astype(BF16)
    vmem = pl.BlockSpec(memory_space=pltpu.VMEM)
    hbm = pl.BlockSpec(memory_space=pl.ANY)
    hid_buf = pltpu.VMEM((rows, tokens), BF16)
    gg, gu, out, squares = pl.pallas_call(
        kernel,
        out_shape=(
            jax.ShapeDtypeStruct((rows, tokens), BF16),
            jax.ShapeDtypeStruct((rows, tokens), BF16),
            jax.ShapeDtypeStruct((rows, cols), F32),
            jax.ShapeDtypeStruct((8, padded), F32),
        ),
        in_specs=[hbm, hbm, vmem, hbm, vmem],
        out_specs=(hbm, hbm, hbm, vmem),
        scratch_shapes=[
            pltpu.VMEM((tokens, width), BF16),
            pltpu.VMEM((5, tokens, cols), BF16),
            pltpu.VMEM((2, tokens, cols // plane), BF16),
            hid_buf, hid_buf, hid_buf,
            pltpu.VMEM((rows, cols), BF16),
            pltpu.VMEM((rows, cols), BF16),
            hid_buf, hid_buf,
            pltpu.VMEM((rows, width), BF16),
            hid_buf, hid_buf,
            pltpu.VMEM((rows, cols), F32),
            pltpu.VMEM((padded, 128), F32),
            pltpu.VMEM((4, 8, padded), F32),
            pltpu.SemaphoreType.DMA((N_SEM,)),
            pltpu.SemaphoreType.DMA((N_SEM,)),
            pltpu.SemaphoreType.DMA((5 + CHUNKS,)),
        ],
        compiler_params=pltpu.CompilerParams(
            collective_id=0, has_side_effects=True, vmem_limit_bytes=67043328),
    )(gate_t, up_t, cotangent, down_weight, hid)
    return gg.T, gu.T, out, squares[0, :rows]


def solution(mesh):
    placed = (
        P("rep", ("fs", "tp")),
        P("rep", ("fs", "tp")),
        P("rep", ("fs", "tp")),
        P(("fs", "tp"), None),
    )
    shape = dict(mesh.shape)
    fits = shape["rep"] // 2 == 2 and shape["fs"] // 2 == 2 and shape["tp"] == 2
    return jax.shard_map(
        fused if fits else local,
        mesh=mesh,
        in_specs=placed,
        out_specs=(
            P("rep", ("fs", "tp")),
            P("rep", ("fs", "tp")),
            P(("fs", "tp"), "rep"),
            P(("fs", "tp")),
        ),
        check_vma=False,
    )
```

time: 195 us -> 126 us (0.65)
  Pallas kernels: 164 us -> 113 us
  blocking collectives: 11.6 us -> 0 us
  local copies, waits for them, and re-layouts: 12.3 us -> 7.33 us
  other arithmetic: 6.53 us -> 3.9 us
    pallas_call x1, Pallas kernels: 164 us -> 113 us  [fused(): pl.pallas_call(kernel, out_shape=(jax.ShapeDtypeStruct((rows, tokens), BF...]
    psum x1 -> x0, blocking collectives: 11.6 us -> none  [fused(): row_squares = lax.psum(jnp.sum(out * out, axis=1), 'rep')]
    unnamed x11 -> x7, local copies, waits for them, and re-layouts: 12.3 us -> 5.86 us
    transpose x1 -> x0, other arithmetic: 4.05 us -> none  [fused(): hid = (g * jax.nn.sigmoid(g) * pre_up.astype(F32)).astype(BF16).T]
    convert_element_type x0 -> x1, other arithmetic: none -> 3.9 us  [fused(): hid = (g * jax.nn.sigmoid(g) * up_t.astype(F32)).astype(BF16)]
    reduce_sum x1 -> x0, other arithmetic: 2.48 us -> none  [fused(): row_squares = lax.psum(jnp.sum(out * out, axis=1), 'rep')]
where the time goes in v2:
time: 126 us; the launch traced here: 125 us
  Pallas kernels  113 us (90%)
  local copies, waits for them, and re-layouts  7.33 us (6%)
  other arithmetic  3.9 us (3%)
    pallas_call x1, Pallas kernels, fused(): pl.pallas_call(kernel, out_shape=(jax.ShapeDtypeStruct((rows, tokens), BF...  113 us
    unnamed x7, local copies, waits for them, and re-layouts  5.86 us
    convert_element_type x1, other arithmetic, fused(): hid = (g * jax.nn.sigmoid(g) * up_t.astype(F32)).astype(BF16)  3.9 us

profile of v2, /device:TPU:0, one launch (start us, length us, event | category | flops | bytes accessed | tf_op | source)
XLA Modules:
  0.0 125.1 jit_solution(556890966939978629)
XLA Ops:
  0.6 3.9 %fusion.4.hid = bf16[992,768]{1,0:T(8,128)(2,1)} fusion(bf16[768,992]{0,1:T(8,128)(2,1)} %param.5, bf16[768,992]{0,1:T(8,128)(2,1)} %param.4), kind=kLoop, calls=%fused_computation.6 | loop fusion | flops 6094848 | bytes 4571136 | tf_op jit(solution)/shard_map/convert_element_type | solution.py:329
  4.5 113.2 %shard_map.75 = (bf16[992,768]{1,0:T(8,128)(2,1)}, bf16[992,768]{1,0:T(8,128)(2,1)}, f32[992,1024]{1,0:T(8,128)}, f32[8,1024]{1,0:T(8,128)}) custom-call(bf16[992,768]{1,0:T(8,128)(2,1)} %bitcast.7, bf16[992,768]{1,0:T(8,128)(2,1)} %bitcast.8, bf16[768,512]{1,0:T(8,128)(2,1)} %shard.1, bf16[992,4096]{1,0:T(8,128)(2,1)} %w_in.1, bf16[992,768]{1,0:T(8,128)(2,1)} %fusion.4.hid), custom_call_target="tpu_custom_call" | custom-call | tf_op jit(solution)/shard_map/pallas_call | solution.py:333
  117.7 0.0 copy-start.1
  117.7 1.5 %slice.3 = f32[1,992]{1,0:T(1,128)} slice(f32[8,1024]{1,0:T(8,128)} %get-tuple-element.11), slice={[0:1], [0:992]} | slice | bytes 7936 | tf_op jit(solution)/shard_map/slice | solution.py:363
  119.2 0.0 copy-start
  119.2 2.8 %copy.11 = bf16[768,992]{0,1:T(8,128)(2,1)} copy(bf16[768,992]{0,1:T(8,128)(2,1)} %bitcast.10) | data formatting | bytes 3047424
  122.0 0.0 copy-done.1
  122.0 1.1 copy.12
  123.1 0.0 copy-done
  123.1 2.0 %copy.13 = f32[992,1024]{1,0:T(8,128)} copy(f32[992,1024]{1,0:T(8,128)S(1)} %copy-done) | data formatting | bytes 8126464
Async XLA Ops:
  117.7 4.2 %copy-start.1 = (bf16[992,768]{1,0:T(8,128)(2,1)S(1)}, bf16[992,768]{1,0:T(8,128)(2,1)}, u32[]{:S(2)}) copy-start(bf16[992,768]{1,0:T(8,128)(2,1)} %get-tuple-element.9) | copy-start | bytes 4571140
  119.2 3.9 %copy-start = (f32[992,1024]{1,0:T(8,128)S(1)}, f32[992,1024]{1,0:T(8,128)}, u32[]{:S(2)}) copy-start(f32[992,1024]{1,0:T(8,128)} %get-tuple-element.18) | copy-start | bytes 12189700

commit v3 on v2

--- a/solution.py
+++ b/solution.py
@@ -48,8 +48,8 @@
     return [(a, min(step, rows - a)) for a in range(0, rows, step)]
 
 
-def kernel(gate_in, up_in, shard, w_in, hid, gg_out, gu_out, out_out, sq_out,
-           G, X, Y, HO, HM, HF, CS, CR, gate, up, w, gg, gu, out, acc, SQ,
+def kernel(gate_in, up_in, shard, w_in, gg_out, gu_out, out_out, sq_out,
+           hid, G, X, Y, HO, HM, HF, CS, CR, gate, up, w, gg, gu, out, acc, SQ,
            ssem, rsem, lsem):
     rep = lax.axis_index("rep")
     fs = lax.axis_index("fs")
@@ -151,23 +151,32 @@
 
     send_plane(OWN, shard, own_view)
 
-    @pl.when(outer)
-    def _():
-        for c in early:
+    loads[0].wait()
+    loads[1].wait()
+
+    def send_hidden(c):
+        @pl.when(outer)
+        def _():
             copy(chunk(hid, c), chunk(HO, c), HO_S + c, (inn, fs, tp)).start()
 
-    @pl.when(inner)
-    def _():
-        for c in early:
+        @pl.when(inner)
+        def _():
             copy(chunk(hid, c), chunk(HM, c), HM_S + c, (mid, fs, tp)).start()
+
+    for c, (a, n) in enumerate(parts):
+        r = pl.ds(a, n)
+        g = gate[r, :].astype(F32)
+        act = g * (1.0 / (1.0 + jnp.exp(-g)))
+        hid[r, :] = (act * up[r, :].astype(F32)).astype(BF16)
+        if c:
+            send_hidden(c - 1)
 
     G[:, at(me * wide, wide)] = shard[...]
     relay_plane(OWN, own_view)
     finish_plane(OWN, own_view)
 
     def hidden_grads():
-        for load in loads:
-            load.wait()
+        loads[2].wait()
         tile = rows // 2
 
         @pl.loop(0, 2)
@@ -307,7 +316,7 @@
     for d in range(1, 4):
         v = SQ.at[(rep + 4 - d) % 4]
         copy(v, v, SQ_S + d - 1, partner).wait_recv()
-    sq_out[...] = (SQ[0] + SQ[1]) + (SQ[2] + SQ[3])
+    sq_out[...] = ((SQ[0] + SQ[1]) + (SQ[2] + SQ[3]))[0:1, :rows]
     for d in range(1, 4):
         copy(SQ.at[rep], SQ.at[rep], SQ_S + d - 1, partner).wait_send()
     sent_plane(OWN, own_view)
@@ -325,8 +334,6 @@
     cols = width // reps
     padded = -(-rows // 128) * 128
     gate_t, up_t = pre_gate.T, pre_up.T
-    g = gate_t.astype(F32)
-    hid = (g * jax.nn.sigmoid(g) * up_t.astype(F32)).astype(BF16)
     vmem = pl.BlockSpec(memory_space=pltpu.VMEM)
     hbm = pl.BlockSpec(memory_space=pl.ANY)
     hid_buf = pltpu.VMEM((rows, tokens), BF16)
@@ -336,11 +343,12 @@
             jax.ShapeDtypeStruct((rows, tokens), BF16),
             jax.ShapeDtypeStruct((rows, tokens), BF16),
             jax.ShapeDtypeStruct((rows, cols), F32),
-            jax.ShapeDtypeStruct((8, padded), F32),
+            jax.ShapeDtypeStruct((1, rows), F32),
         ),
-        in_specs=[hbm, hbm, vmem, hbm, vmem],
+        in_specs=[hbm, hbm, vmem, hbm],
         out_specs=(hbm, hbm, hbm, vmem),
         scratch_shapes=[
+            hid_buf,
             pltpu.VMEM((tokens, width), BF16),
             pltpu.VMEM((5, tokens, cols), BF16),
             pltpu.VMEM((2, tokens, cols // plane), BF16),
@@ -359,8 +367,8 @@
         ],
         compiler_params=pltpu.CompilerParams(
             collective_id=0, has_side_effects=True, vmem_limit_bytes=67043328),
-    )(gate_t, up_t, cotangent, down_weight, hid)
-    return gg.T, gu.T, out, squares[0, :rows]
+    )(gate_t, up_t, cotangent, down_weight)
+    return gg.T, gu.T, out, squares.reshape(rows)
 
 
 def solution(mesh):

time: 126 us -> 122 us (0.968)
  other arithmetic: 3.9 us -> 0 us
    convert_element_type x1 -> x0, other arithmetic: 3.9 us -> none  [fused(): hid = (g * jax.nn.sigmoid(g) * up_t.astype(F32)).astype(BF16)]
    unnamed x7 -> x8, local copies, waits for them, and re-layouts: 5.86 us -> 7.95 us
    slice x1 -> x0, local copies, waits for them, and re-layouts: 1.47 us -> none  [fused(): return (gg.T, gu.T, out, squares[0, :rows])]
where the time goes in v3:
time: 122 us; the launch traced here: 121 us
  Pallas kernels  113 us (93%)
  local copies, waits for them, and re-layouts  7.95 us (7%)
    pallas_call x1, Pallas kernels, fused(): pl.pallas_call(kernel, out_shape=(jax.ShapeDtypeStruct((rows, tokens), BF...  113 us
    unnamed x8, local copies, waits for them, and re-layouts  7.95 us

profile of v3, /device:TPU:0, one launch (start us, length us, event | category | flops | bytes accessed | tf_op | source)
XLA Modules:
  0.0 121.2 jit_solution(2207287773093597278)
XLA Ops:
  0.6 112.6 %shard_map.75 = (bf16[992,768]{1,0:T(8,128)(2,1)}, bf16[992,768]{1,0:T(8,128)(2,1)}, f32[992,1024]{1,0:T(8,128)}, f32[1,992]{1,0:T(1,128)}) custom-call(bf16[992,768]{1,0:T(8,128)(2,1)} %bitcast.7, bf16[992,768]{1,0:T(8,128)(2,1)} %bitcast.8, bf16[768,512]{1,0:T(8,128)(2,1)} %shard.1, bf16[992,4096]{1,0:T(8,128)(2,1)} %w_in.1), custom_call_target="tpu_custom_call" | custom-call | tf_op jit(solution)/shard_map/pallas_call | solution.py:340
  113.3 0.0 copy-start
  113.3 2.8 %copy.12 = bf16[768,992]{0,1:T(8,128)(2,1)} copy(bf16[768,992]{0,1:T(8,128)(2,1)} %bitcast.6) | data formatting | bytes 3047424
  116.0 2.6 %copy.13 = bf16[768,992]{0,1:T(8,128)(2,1)} copy(bf16[768,992]{0,1:T(8,128)(2,1)} %bitcast.5) | data formatting | bytes 3047424
  118.7 0.0 copy-done
  118.7 0.0 copy-start.1
  118.7 2.0 %copy.14 = f32[992,1024]{1,0:T(8,128)} copy(f32[992,1024]{1,0:T(8,128)S(1)} %copy-done) | data formatting | bytes 8126464
  120.6 0.0 copy-done.1
  120.6 0.6 copy.15
Async XLA Ops:
  113.3 5.4 %copy-start = (f32[992,1024]{1,0:T(8,128)S(1)}, f32[992,1024]{1,0:T(8,128)}, u32[]{:S(2)}) copy-start(f32[992,1024]{1,0:T(8,128)} %get-tuple-element.18) | copy-start | bytes 12189700
  118.7 2.0 %copy-start.1 = (f32[1,992]{1,0:T(1,128)S(1)}, f32[1,992]{1,0:T(1,128)}, u32[]{:S(2)}) copy-start(f32[1,992]{1,0:T(1,128)} %get-tuple-element.11) | copy-start | bytes 11908
